TPU v7x, 256 devices: a whole 4x4x8 slice. The times are simulated.
256 devices in a mesh: sp: 32 (over z, y), tp: 8 (over x, core).
Axes of the slice: x: 4, y: 4, z: 8, core: 2. Of those that a mesh axis runs over, the one named last changes fastest.
Arguments:
- skip_stream: bfloat16 [24576, 2048], P(('sp', 'tp')), may hold values from -24 to 24
- acceptance_signal: bfloat16 [24576, 2048], P('sp', 'tp'), may hold values from -6 to 6
- lookup_mapped: bfloat16 [24576, 2048], P('sp', 'tp'), may hold values from -12 to 12
- payload_mapped: bfloat16 [24576, 2048], P('sp', 'tp'), may hold values from -6 to 6
- result_switch: bfloat16 [24576, 2048], P('sp', 'tp'), may hold values from -6 to 6
- forget_dynamic_share: bfloat16 [24576, 2048], P('sp', 'tp'), may hold values from -4 to 4
- additive_forget_logarithm: float32 [24576, 32], P('sp', 'tp'), may hold values from -1 to 0
- forget_feature_offset: float32 [2048], P('tp'), may hold values from -11 to -3
- substitution_dynamic_share: bfloat16 [24576, 2048], P('sp', 'tp'), may hold values from -6 to 6
- substitution_feature_offset: float32 [2048], P('tp'), may hold values from -6.5 to 2.5
- diagonal_reward_scales: float32 [2048], P('tp'), may hold values from -0.9 to 0.9
- result_matrix: bfloat16 [2048, 2048], P('tp'), may hold values from -0.125 to 0.125
- mlp_rescaler: float32 [2048], replicated, may hold values from 0.1 to 1.9
- switch_matrix: bfloat16 [2048, 5120], P('sp', 'tp'), may hold values from -0.125 to 0.125
- expand_matrix: bfloat16 [2048, 5120], P('sp', 'tp'), may hold values from -0.125 to 0.125
- contract_matrix: bfloat16 [2048, 5120], P('sp', 'tp'), may hold values from -0.25 to 0.25
Outputs:
- mixed_out: bfloat16 [24576, 2048], P(('sp', 'tp'))
All inputs are finite; a program needn't handle non-finite values.
Results may differ from a plain program's by a relative error of at most 0.015.
Values may be sent and summed in bfloat16 or wider, within the bound.
A program may use at most 128 MiB of HBM per device.

v0:
```python
import jax
import jax.numpy as jnp
from jax import lax
from jax.sharding import Mesh
from jax.sharding import PartitionSpec as P

PER_GROUP_DIMS = 64
SP = ("sp_0", "sp_1")
SP_TP = ("sp_0", "sp_1", "tp")
norm_eps = 1e-06
group_eps = 0.00064
half_step = 0.5


def side_by_side(arrays, axis, dim, along):
    widths = [a.shape[along] for a in arrays]
    both = jnp.concatenate(arrays, axis=along)
    result = lax.all_gather(both, axis, axis=dim, tiled=True)
    return tuple(jnp.split(result, [sum(widths[:k]) for k in range(1, len(widths))], axis=along))


def filled_with(shard, identity):
    return jax.tree.map(
        lambda a, e: jnp.broadcast_to(jnp.asarray(e, a.dtype), a.shape), shard, identity
    )


def carried_in(shard, axes, combine, identity):
    before = start = filled_with(shard, identity)
    so_far = shard
    for axis in reversed(axes):
        peers, place = (lax.axis_size(axis), lax.axis_index(axis))
        pieces = jax.tree.map(
            lambda part, kind: lax.all_gather(part.astype(kind), axis),
            so_far,
            (jnp.bfloat16, jnp.bfloat16),
        )
        inside, so_far = (start, start)
        for k in range(peers):
            passed = k < place
            so_far = combine(
                so_far, jax.tree.map(lambda part, own: part[k].astype(own.dtype), pieces, shard)
            )
            inside = jax.tree.map(lambda new, old: jnp.where(passed, new, old), so_far, inside)
        before = combine(inside, before)
    return before


def split_up(shard, dim, peers):
    before, after = (shard.shape[:dim], shard.shape[dim + 1 :])
    return jnp.moveaxis(shard.reshape(*before, peers, -1, *after), dim, 0)


def sent_and_summed(shard, axis, dim):
    peers = lax.axis_size(axis)
    parts = lax.all_to_all(split_up(shard, dim, peers), axis, 0, 0, tiled=True)
    return jnp.sum(parts.astype(jnp.float32), axis=0)


def compose(earlier, latter):
    prod_first, carry_first = earlier
    prod_second, carry_second = latter
    product = jnp.einsum("hij,hjk->hik", prod_first, prod_second)
    carried = jnp.einsum("hij,hjk->hik", carry_first, prod_second) + carry_second
    return (product, carried)


def masked_pairs(left, right, keep):
    return jnp.where(keep, jnp.einsum("htc,hjc->htj", left, right), 0.0)


def block_step(carry, inputs):
    state_part, transition = carry
    read_blk, logstep_blk, key_blk, value_blk, unit_blk, rate_blk = inputs
    length = read_blk.shape[1]
    width = value_blk.shape[2]
    cumulate = jnp.cumsum(logstep_blk, axis=1)
    growth = jnp.exp(cumulate)
    shrink = jnp.exp(-cumulate)
    before_unit = jnp.exp(cumulate - logstep_blk) * unit_blk
    erase_dir = unit_blk * rate_blk
    key_back = key_blk * shrink
    erase_back = erase_dir * shrink
    read_fwd = read_blk * growth
    end_growth = growth[:, -1:, :]
    key_end = key_back * end_growth
    erase_end = erase_back * end_growth
    row_index = lax.broadcasted_iota(jnp.int32, (length, length), 0)
    col_index = lax.broadcasted_iota(jnp.int32, (length, length), 1)
    strict = col_index < row_index
    inclusive = col_index <= row_index
    key_past = masked_pairs(before_unit, key_back, strict)
    erase_past = masked_pairs(before_unit, erase_back, strict)
    key_read = masked_pairs(read_fwd, key_back, inclusive)
    erase_read = masked_pairs(read_fwd, erase_back, inclusive)
    recall_rhs = jnp.einsum("htk,hvk->htv", before_unit, state_part) + jnp.einsum(
        "htj,hjv->htv", key_past, value_blk
    )
    solved = jax.scipy.linalg.solve_triangular(
        erase_past,
        jnp.concatenate([recall_rhs, before_unit], axis=-1),
        lower=True,
        unit_diagonal=True,
    )
    recalled = solved[..., :width]
    carried_map = solved[..., width:]
    local_out = (
        jnp.einsum("htk,hvk->htv", read_fwd, state_part)
        + jnp.einsum("htj,hjv->htv", key_read, value_blk)
        - jnp.einsum("htj,hjv->htv", erase_read, recalled)
    )
    from_start = read_fwd - jnp.einsum("htj,hjk->htk", erase_read, carried_map)
    coefficient = jnp.einsum("htk,hjk->htj", from_start, transition)
    new_state = (
        state_part * end_growth
        + jnp.einsum("htv,htk->hvk", value_blk, key_end)
        - jnp.einsum("htv,htk->hvk", recalled, erase_end)
    )
    step_map = jnp.eye(width, dtype=jnp.float32)[None] * end_growth - jnp.einsum(
        "htj,htk->hjk", carried_map, erase_end
    )
    new_transition = jnp.einsum("hij,hjk->hik", transition, step_map)
    return ((new_state, new_transition), (local_out, coefficient))


def per_device(
    skip_stream,
    acceptance_signal,
    lookup_mapped,
    payload_mapped,
    result_switch,
    forget_dynamic_share,
    additive_forget_logarithm,
    forget_feature_offset,
    substitution_dynamic_share,
    substitution_feature_offset,
    diagonal_reward_scales,
    result_matrix,
    mlp_rescaler,
    switch_matrix,
    expand_matrix,
    contract_matrix,
):
    matrix_length, matrix_breadth = acceptance_signal.shape
    attention_groups = matrix_breadth // PER_GROUP_DIMS
    gate_whole, up_whole, down_whole = side_by_side(
        (switch_matrix, expand_matrix, contract_matrix), SP, 0, 1
    )

    def by_head(values):
        return values.astype(jnp.float32).reshape(matrix_length, attention_groups, PER_GROUP_DIMS)

    acceptance_lines = by_head(acceptance_signal)
    lookup_vectors = by_head(lookup_mapped)
    payload_vectors = by_head(payload_mapped)
    log_decay_rate = (
        -jax.nn.softplus(
            -(forget_feature_offset[None, :] + forget_dynamic_share.astype(jnp.float32))
        )
        - 0.5
    )
    log_step = (
        -jnp.exp(log_decay_rate).reshape(matrix_length, attention_groups, PER_GROUP_DIMS)
        + additive_forget_logarithm[:, :, None]
    )
    replace_rate = jax.nn.sigmoid(
        substitution_feature_offset[None, :] + substitution_dynamic_share.astype(jnp.float32)
    )
    replace_rate = replace_rate.reshape(matrix_length, attention_groups, PER_GROUP_DIMS)
    unit_key = lookup_vectors * lax.rsqrt(
        jnp.sum(lookup_vectors * lookup_vectors, axis=-1, keepdims=True) + norm_eps
    )
    block_len = min(64, matrix_length)
    block_count = matrix_length // block_len

    def to_blocks(values):
        return values.reshape(block_count, block_len, attention_groups, PER_GROUP_DIMS).transpose(
            0, 2, 1, 3
        )

    def from_blocks(values):
        return values.transpose(0, 2, 1, 3).reshape(matrix_length, attention_groups, PER_GROUP_DIMS)

    identity_mats = jnp.broadcast_to(
        jnp.eye(PER_GROUP_DIMS, dtype=jnp.float32),
        (attention_groups, PER_GROUP_DIMS, PER_GROUP_DIMS),
    )
    zero_mats = jnp.zeros((attention_groups, PER_GROUP_DIMS, PER_GROUP_DIMS), jnp.float32)
    (closing_state, closing_map), (local_blocks, coef_blocks) = lax.scan(
        block_step,
        (zero_mats, identity_mats),
        (
            to_blocks(acceptance_lines),
            to_blocks(log_step),
            to_blocks(lookup_vectors),
            to_blocks(payload_vectors),
            to_blocks(unit_key),
            to_blocks(replace_rate),
        ),
    )
    _, carried = carried_in((closing_map, closing_state), SP, compose, (identity_mats, zero_mats))
    outcome = from_blocks(local_blocks) + jnp.einsum(
        "hvk,thk->thv", carried, from_blocks(coef_blocks)
    )
    centre = jnp.mean(outcome, axis=-1, keepdims=True)
    spread = jnp.mean(jnp.square(outcome - centre), axis=-1, keepdims=True)
    rescaled_attention = (outcome - centre) * lax.rsqrt(spread + group_eps)
    diagonal_reward_summand = (
        jnp.sum(
            acceptance_lines
            * lookup_vectors
            * diagonal_reward_scales.reshape(attention_groups, PER_GROUP_DIMS),
            axis=-1,
            keepdims=True,
        )
        * payload_vectors
    )
    merged_attention = (
        (rescaled_attention + diagonal_reward_summand).reshape(matrix_length, matrix_breadth)
        * result_switch.astype(jnp.float32)
    ).astype(jnp.bfloat16)
    row_block = merged_attention
    projected = sent_and_summed(
        jnp.dot(row_block, result_matrix, preferred_element_type=jnp.float32).astype(jnp.bfloat16),
        "tp",
        0,
    ).astype(jnp.bfloat16)
    stream = skip_stream.astype(jnp.float32) + lax.optimization_barrier(projected).astype(
        jnp.float32
    )
    scale_rows = lax.rsqrt(jnp.mean(stream * stream, axis=-1, keepdims=True) + norm_eps)
    normed_rows = (stream * scale_rows * mlp_rescaler[None, :]).astype(jnp.bfloat16)
    whole_rows = lax.all_gather(normed_rows, "tp", axis=0, tiled=True)
    gate_act = jnp.dot(whole_rows, gate_whole, preferred_element_type=jnp.float32)
    up_act = jnp.dot(whole_rows, up_whole, preferred_element_type=jnp.float32)
    hidden = (jax.nn.silu(gate_act) * up_act).astype(jnp.bfloat16)
    row_block = hidden
    ffn_out = lax.psum_scatter(
        lax.dot_general(
            row_block, down_whole, (((1,), (1,)), ((), ())), preferred_element_type=jnp.float32
        ).astype(jnp.bfloat16),
        "tp",
        scatter_dimension=0,
        tiled=True,
    )
    return (stream + half_step * lax.optimization_barrier(ffn_out).astype(jnp.float32)).astype(
        jnp.bfloat16
    )


def solution(mesh):
    torus = Mesh(mesh.devices.reshape(8, 4, mesh.shape["tp"]), ("sp_0", "sp_1", "tp"))
    in_specs = (
        P(SP_TP, None),
        P(SP, "tp"),
        P(SP, "tp"),
        P(SP, "tp"),
        P(SP, "tp"),
        P(SP, "tp"),
        P(SP, "tp"),
        P("tp"),
        P(SP, "tp"),
        P("tp"),
        P("tp"),
        P("tp", None),
        P(),
        P(SP, "tp"),
        P(SP, "tp"),
        P(SP, "tp"),
    )
    out_specs = P(SP_TP, None)
    return jax.shard_map(
        per_device, mesh=torus, in_specs=in_specs, out_specs=out_specs, check_vma=False
    )
```

profile of v0, /device:TPU:8, one launch (start us, length us, event | category | flops | bytes accessed | tf_op | source)
XLA Modules:
  0.0 707.8 jit_solution(7916593708579089121)
XLA Ops:
  6.5 1.3 copy.62
  10.1 2.5 reshape_reshape.12
  12.6 2.1 copy.77
  14.7 1.8 reshape_reshape.13
  17.5 1.5 fusion.80
  19.0 1.9 neg.31
  20.9 1.7 copy.87
  23.3 1.8 reshape_reshape.15
  25.1 1.2 add_divide_fusion
  26.3 1.9 reshape_reshape.14
  28.2 4.9 multiply_bitcast_fusion
  33.1 339.6 %while.17 = (s32[]{:T(128)}, f32[4,64,64]{2,1,0:T(8,128)S(1)}, bf16[4,64,64]{1,2,0:T(8,128)(2,1)S(1)}, f32[12,4,64,64]{3,2,1,0:T(8,128)}, bf16[12,4,64,64]{3,2,1...) while((s32[]{:T(128)}, f32[4,64,64]{2,1,0:T(8,128)S(1)}, ...), condition=%wide.region_3.4_spmd.clone, body=%wide.region_1.3_spmd.clone.sunk | while | flops 58290240 | bytes 4974245 | solution.py:189
  35.2 1.0 constant_dynamic-slice_fusion.12
  38.1 19.7 %custom-call.9 = f32[4,1,64,64]{2,3,1,0:T(8,128)S(1)} custom-call(f32[4,1,64,64]{3,2,1,0:T(8,128)S(1)} %fusion.259), custom_call_target="InvertDiagBlocksLowerTriangular" | custom-call | tf_op jit(solution)/shard_map/while/body/eval_jaxpr/jit(_solve_triangular)/vmap()/triangular_solve | solution.py:99
  63.5 1.0 constant_dynamic-slice_fusion.12
  66.4 19.7 %custom-call.9 = f32[4,1,64,64]{2,3,1,0:T(8,128)S(1)} custom-call(f32[4,1,64,64]{3,2,1,0:T(8,128)S(1)} %fusion.259), custom_call_target="InvertDiagBlocksLowerTriangular" | custom-call | tf_op jit(solution)/shard_map/while/body/eval_jaxpr/jit(_solve_triangular)/vmap()/triangular_solve | solution.py:99
  91.8 1.0 constant_dynamic-slice_fusion.12
  94.7 19.7 %custom-call.9 = f32[4,1,64,64]{2,3,1,0:T(8,128)S(1)} custom-call(f32[4,1,64,64]{3,2,1,0:T(8,128)S(1)} %fusion.259), custom_call_target="InvertDiagBlocksLowerTriangular" | custom-call | tf_op jit(solution)/shard_map/while/body/eval_jaxpr/jit(_solve_triangular)/vmap()/triangular_solve | solution.py:99
  120.1 1.0 constant_dynamic-slice_fusion.12
  123.0 19.7 %custom-call.9 = f32[4,1,64,64]{2,3,1,0:T(8,128)S(1)} custom-call(f32[4,1,64,64]{3,2,1,0:T(8,128)S(1)} %fusion.259), custom_call_target="InvertDiagBlocksLowerTriangular" | custom-call | tf_op jit(solution)/shard_map/while/body/eval_jaxpr/jit(_solve_triangular)/vmap()/triangular_solve | solution.py:99
  151.3 19.7 %custom-call.9 = f32[4,1,64,64]{2,3,1,0:T(8,128)S(1)} custom-call(f32[4,1,64,64]{3,2,1,0:T(8,128)S(1)} %fusion.259), custom_call_target="InvertDiagBlocksLowerTriangular" | custom-call | tf_op jit(solution)/shard_map/while/body/eval_jaxpr/jit(_solve_triangular)/vmap()/triangular_solve | solution.py:99
  179.6 19.7 %custom-call.9 = f32[4,1,64,64]{2,3,1,0:T(8,128)S(1)} custom-call(f32[4,1,64,64]{3,2,1,0:T(8,128)S(1)} %fusion.259), custom_call_target="InvertDiagBlocksLowerTriangular" | custom-call | tf_op jit(solution)/shard_map/while/body/eval_jaxpr/jit(_solve_triangular)/vmap()/triangular_solve | solution.py:99
  207.9 19.7 %custom-call.9 = f32[4,1,64,64]{2,3,1,0:T(8,128)S(1)} custom-call(f32[4,1,64,64]{3,2,1,0:T(8,128)S(1)} %fusion.259), custom_call_target="InvertDiagBlocksLowerTriangular" | custom-call | tf_op jit(solution)/shard_map/while/body/eval_jaxpr/jit(_solve_triangular)/vmap()/triangular_solve | solution.py:99
  236.2 19.7 %custom-call.9 = f32[4,1,64,64]{2,3,1,0:T(8,128)S(1)} custom-call(f32[4,1,64,64]{3,2,1,0:T(8,128)S(1)} %fusion.259), custom_call_target="InvertDiagBlocksLowerTriangular" | custom-call | tf_op jit(solution)/shard_map/while/body/eval_jaxpr/jit(_solve_triangular)/vmap()/triangular_solve | solution.py:99
  264.5 19.7 %custom-call.9 = f32[4,1,64,64]{2,3,1,0:T(8,128)S(1)} custom-call(f32[4,1,64,64]{3,2,1,0:T(8,128)S(1)} %fusion.259), custom_call_target="InvertDiagBlocksLowerTriangular" | custom-call | tf_op jit(solution)/shard_map/while/body/eval_jaxpr/jit(_solve_triangular)/vmap()/triangular_solve | solution.py:99
  292.8 19.7 %custom-call.9 = f32[4,1,64,64]{2,3,1,0:T(8,128)S(1)} custom-call(f32[4,1,64,64]{3,2,1,0:T(8,128)S(1)} %fusion.259), custom_call_target="InvertDiagBlocksLowerTriangular" | custom-call | tf_op jit(solution)/shard_map/while/body/eval_jaxpr/jit(_solve_triangular)/vmap()/triangular_solve | solution.py:99
  321.1 19.7 %custom-call.9 = f32[4,1,64,64]{2,3,1,0:T(8,128)S(1)} custom-call(f32[4,1,64,64]{3,2,1,0:T(8,128)S(1)} %fusion.259), custom_call_target="InvertDiagBlocksLowerTriangular" | custom-call | tf_op jit(solution)/shard_map/while/body/eval_jaxpr/jit(_solve_triangular)/vmap()/triangular_solve | solution.py:99
  349.4 19.7 %custom-call.9 = f32[4,1,64,64]{2,3,1,0:T(8,128)S(1)} custom-call(f32[4,1,64,64]{3,2,1,0:T(8,128)S(1)} %fusion.259), custom_call_target="InvertDiagBlocksLowerTriangular" | custom-call | tf_op jit(solution)/shard_map/while/body/eval_jaxpr/jit(_solve_triangular)/vmap()/triangular_solve | solution.py:99
  372.8 12.5 %all-gather = bf16[16,64,64]{2,1,0:T(8,128)(2,1)S(1)} all-gather(bf16[4,64,64]{2,1,0:T(8,128)(2,1)S(1)} %copy.76), channel_id=2, replica_groups=mesh['sp_0'=8,'sp_1'=4,'tp'=8] {'sp_1'}, dimensions={0}, use_global_device_ids=true | all-gather | bytes 163840 | tf_op jit(solution)/shard_map/all_gather | solution.py:34
  385.3 12.3 %all-gather.2 = bf16[16,64,64]{2,1,0:T(8,128)(2,1)S(1)} all-gather(bf16[4,64,64]{2,1,0:T(8,128)(2,1)S(1)} %convert_element_type.170), channel_id=4, replica_groups=mesh['sp_0'=8,'sp_1'=4,'tp'=8] {'sp_1'}, dimensions={0}, use_global_device_ids=true | all-gather | bytes 163840 | tf_op jit(solution)/shard_map/all_gather | solution.py:34
  400.0 29.3 %all-gather.3 = bf16[32,64,64]{2,1,0:T(8,128)(2,1)S(1)} all-gather(bf16[4,64,64]{2,1,0:T(8,128)(2,1)S(1)} %convolution_add_fusion.10), channel_id=5, replica_groups=mesh['sp_0'=8,'sp_1'=4,'tp'=8] {'sp_0'}, dimensions={0}, use_global_device_ids=true | all-gather | bytes 294912 | tf_op jit(solution)/shard_map/all_gather | solution.py:34
  430.4 25.5 %all-gather.1 = bf16[32,64,64]{2,1,0:T(8,128)(2,1)S(1)} all-gather(bf16[4,64,64]{2,1,0:T(8,128)(2,1)S(1)} %fusion.143), channel_id=3, replica_groups=mesh['sp_0'=8,'sp_1'=4,'tp'=8] {'sp_0'}, dimensions={0}, use_global_device_ids=true | all-gather | bytes 294912 | tf_op jit(solution)/shard_map/all_gather | solution.py:34
  459.5 2.2 copy.74
  461.7 1.4 reshape.103
  463.1 1.9 copy.75
  465.0 1.4 reshape.104
  466.6 2.0 fusion.73
  468.6 1.6 fusion.160
  470.4 1.1 fusion.68
  471.6 1.4 copy.78
  474.0 42.6 %all_to_all.5 = bf16[8,96,2048]{2,1,0:T(8,128)(2,1)} all-to-all(bf16[8,96,2048]{2,1,0:T(8,128)(2,1)S(1)} %bitcast.166), channel_id=1, replica_groups=mesh['sp_0'=8,'sp_1'=4,'tp'=8] {'tp'}, dimensions={0} | all-to-all | bytes 6291456 | tf_op jit(solution)/shard_map/all_to_all | solution.py:56
  516.7 2.5 reduce_sum.61
  521.5 26.1 %all-gather.7.cloned.1.call-done = bf16[768,2048]{1,0:T(8,128)(2,1)} async-done(((bf16[96,2048]{1,0:T(8,128)(2,1)}), bf16[768,2048]{1,0:T(8,128)(2,1)}) %all-gather.7.cloned.1.call-update) | async-done | bytes 3145744 | tf_op jit(solution)/shard_map/all_gather | solution.py:233
  547.6 96.5 %all-gather.9.cloned.1.call-done = bf16[2048,1920]{1,0:T(8,128)(2,1)} async-done(((bf16[64,1920]{1,0:T(8,128)(2,1)}), bf16[2048,1920]{1,0:T(8,128)(2,1)}) %all-gather.9.cloned.1.call-update) | async-done | bytes 7864336 | tf_op jit(solution)/shard_map/all_gather | solution.py:18
  644.2 6.6 fusion.62
  650.8 11.6 %convolution_convert_fusion = bf16[768,2048]{1,0:T(8,128)(2,1)} fusion(bf16[2048,1920]{1,0:T(8,128)(2,1)} %all-gather.9.cloned.1.call-done, f32[768,640]{1,0:T(8,128)} %fusion.62, bf16[768,2048]{1,0:T(8,128)(2,1)} %all-gather.7.cloned.1.call-done), kind=kOutput, calls=%fused_computation.82 | convolution fusion | flops 4031053824 | bytes 13500416 | tf_op jit(solution)/shard_map/dot_general | solution.py:239
  662.4 37.0 %reduce-scatter.2.cloned.1.call-done = bf16[96,2048]{1,0:T(8,128)(2,1)} async-done(((bf16[768,2048]{1,0:T(8,128)(2,1)}), bf16[96,2048]{1,0:T(8,128)(2,1)}) %reduce-scatter.2.cloned.1.call-update) | async-done | bytes 393232 | tf_op jit(solution)/shard_map/reduce_scatter | solution.py:238
  699.4 1.9 add_convert_fusion
  (428 shorter events, 112.5 us)
Async XLA Ops:
  6.5 466.5 %copy-start = (bf16[256,2048]{1,0:T(8,128)(2,1)S(1)}, bf16[256,2048]{1,0:T(8,128)(2,1)}, u32[]{:S(2)}) copy-start(bf16[256,2048]{1,0:T(8,128)(2,1)} %param.29) | copy-start | bytes 3145732
  6.5 2.2 copy-start.7
  6.5 541.1 %all-gather.7.cloned.1.call-start = ((), (), s32[]{:S(2)}) async-start(), calls=%async_computation.2 | async-start | bytes 3538944 | tf_op jit(solution)/shard_map/all_gather | solution.py:233
  12.6 3.9 copy-start.27
  12.6 4.9 copy-start.8
  12.6 4.9 copy-start.30
  28.1 4.9 copy-start.23
  397.7 31.9 %copy-start.10 = (bf16[4,64,64]{2,1,0:T(8,128)(2,1)}, bf16[4,64,64]{2,1,0:T(8,128)(2,1)S(1)}, u32[]{:S(2)}) copy-start(bf16[4,64,64]{2,1,0:T(8,128)(2,1)S(1)} %fusion.116) | copy-start | bytes 98308
  397.9 0.6 copy-start.25
  398.6 0.6 copy-start.16
  399.2 0.6 copy-start.18
  429.3 28.8 %copy-start.4 = (bf16[32,64,64]{2,1,0:T(8,128)(2,1)}, bf16[32,64,64]{2,1,0:T(8,128)(2,1)S(1)}, u32[]{:S(2)}) copy-start(bf16[32,64,64]{2,1,0:T(8,128)(2,1)S(1)} %all-gather.3) | copy-start | bytes 786436
  429.8 0.6 copy-start.9
  455.9 2.2 copy-start.5
  456.0 0.7 copy-start.24
  456.8 4.8 copy-start.11
  457.0 4.7 copy-start.12
  457.2 4.5 copy-start.13
  457.3 0.6 copy-start.14
  458.1 0.6 copy-start.15
  463.1 3.3 copy-start.17
  463.1 3.3 copy-start.19
  463.1 3.3 copy-start.26
  466.6 3.8 copy-start.2
  466.6 3.8 copy-start.3
  468.6 1.7 copy-start.29
  471.6 1.5 copy-start.6
  516.7 2.5 copy-start.1
  516.7 2.8 copy-start.28
  519.2 1.3 copy-start.20
  519.2 1.3 copy-start.21
  519.2 1.3 copy-start.22
  520.4 123.8 %all-gather.9.cloned.1.call-start = ((), (), s32[]{:S(2)}) async-start(), calls=%async_computation.3 | async-start | bytes 8110080 | tf_op jit(solution)/shard_map/all_gather | solution.py:18
  521.2 178.2 %reduce-scatter.2.cloned.1.call-start = ((), (), s32[]{:S(2)}) async-start(), calls=%async_computation.4 | async-start | bytes 3538944 | tf_op jit(solution)/shard_map/reduce_scatter | solution.py:238
Sparse Core Ops, SparseCore 0:
  520.5 27.0 all-gather.6
  550.2 93.9 all-gather.8
  662.5 36.8 reduce-scatter.1
where the time goes:
time: 710 us; the launch traced here: 708 us
  other arithmetic  257 us (36%)
  waiting for transfers between devices  160 us (23%)
  blocking collectives  122 us (17%)
  matrix products  76.9 us (11%)
  local copies, waits for them, and re-layouts  76.8 us (11%)
  between operations  13.5 us (2%)
    another operation x36, other arithmetic, block_step(): jax.scipy.linalg.solve_triangular(erase_past, jnp.concatenate([recall_rhs...  236 us
    all_gather x1, waiting for transfers between devices, side_by_side(): result = lax.all_gather(both, axis, axis=dim, tiled=True)  96.5 us
    all_gather x4, blocking collectives, carried_in(): lax.all_gather(part.astype(kind), axis)  79.6 us
    dynamic_slice x72, local copies, waits for them, and re-layouts, per_device(): lax.scan(block_step, (zero_mats, identity_mats), (to_blocks(acceptance_li...  46.8 us
    all_to_all x1, blocking collectives, sent_and_summed(): parts = lax.all_to_all(split_up(shard, dim, peers), axis, 0, 0, tiled=True)  42.6 us
    reduce_scatter x1, waiting for transfers between devices, per_device(): lax.psum_scatter(lax.dot_general(row_block, down_whole, (((1,), (1,)), ((...  37 us
    all_gather x1, waiting for transfers between devices, per_device(): whole_rows = lax.all_gather(normed_rows, 'tp', axis=0, tiled=True)  26.1 us
  transfers between devices with their start and end apart: 3, of which 3 were waited for; matrix products, arithmetic and copies ran while one was open for 0% of the time, Pallas kernels for 0%

commit v1 on v0

--- a/solution.py
+++ b/solution.py
@@ -230,7 +230,9 @@
     )
     scale_rows = lax.rsqrt(jnp.mean(stream * stream, axis=-1, keepdims=True) + norm_eps)
     normed_rows = (stream * scale_rows * mlp_rescaler[None, :]).astype(jnp.bfloat16)
-    whole_rows = lax.all_gather(normed_rows, "tp", axis=0, tiled=True)
+    whole_rows = jnp.concatenate(
+        lax.all_to_all(jnp.stack([normed_rows] * lax.axis_size("tp")), "tp", 0, 0), axis=0
+    )
     gate_act = jnp.dot(whole_rows, gate_whole, preferred_element_type=jnp.float32)
     up_act = jnp.dot(whole_rows, up_whole, preferred_element_type=jnp.float32)
     hidden = (jax.nn.silu(gate_act) * up_act).astype(jnp.bfloat16)

time: 710 us -> 628 us (0.88)
  waiting for transfers between devices: 160 us -> 35.8 us
  blocking collectives: 122 us -> 164 us
    all_gather x1, waiting for transfers between devices: 96.5 us -> 0.01 us  [side_by_side(): result = lax.all_gather(both, axis, axis=dim, tiled=True)]
    all_to_all x0 -> x1, blocking collectives: none -> 41.7 us  [per_device(): lax.all_to_all(jnp.stack([normed_rows] * lax.axis_size('tp')), 'tp', 0, 0)]
    all_gather x1 -> x0, waiting for transfers between devices: 26.1 us -> none  [per_device(): whole_rows = lax.all_gather(normed_rows, 'tp', axis=0, tiled=True)]
  transfers between devices with their start and end apart: 3 -> 2, of which waited for: 3 -> 1; matrix products, arithmetic and copies ran while one was open for 0% -> 62% of each run, Pallas kernels for 0% -> 0%
where the time goes in v1:
time: 628 us; the launch traced here: 626 us
  other arithmetic  256 us (41%)
  blocking collectives  164 us (26%)
  local copies, waits for them, and re-layouts  77.2 us (12%)
  matrix products  77.1 us (12%)
  waiting for transfers between devices  35.8 us (6%)
  between operations  13.9 us (2%)
    another operation x36, other arithmetic, block_step(): jax.scipy.linalg.solve_triangular(erase_past, jnp.concatenate([recall_rhs...  236 us
    all_gather x4, blocking collectives, carried_in(): lax.all_gather(part.astype(kind), axis)  79.5 us
    dynamic_slice x72, local copies, waits for them, and re-layouts, per_device(): lax.scan(block_step, (zero_mats, identity_mats), (to_blocks(acceptance_li...  46.8 us
    all_to_all x1, blocking collectives, sent_and_summed(): parts = lax.all_to_all(split_up(shard, dim, peers), axis, 0, 0, tiled=True)  42.6 us
    all_to_all x1, blocking collectives, per_device(): lax.all_to_all(jnp.stack([normed_rows] * lax.axis_size('tp')), 'tp', 0, 0)  41.7 us
    reduce_scatter x1, waiting for transfers between devices, per_device(): lax.psum_scatter(lax.dot_general(row_block, down_whole, (((1,), (1,)), ((...  35.8 us
  transfers between devices with their start and end apart: 2, of which 1 were waited for; matrix products, arithmetic and copies ran while one was open for 62% of the time, Pallas kernels for 0%

profile of v1, /device:TPU:8, one launch (start us, length us, event | category | flops | bytes accessed | tf_op | source)
XLA Modules:
  0.0 625.9 jit_solution(9580218652307525913)
XLA Ops:
  6.5 1.8 pad_maximum_fusion
  8.4 1.2 copy.62
  9.9 1.9 reshape_reshape.13
  12.8 1.5 fusion.80
  14.3 1.9 neg.31
  17.9 1.2 copy.65
  19.0 1.1 copy.66
  20.1 2.9 reshape_reshape.15
  23.0 2.1 add_divide_fusion
  25.1 2.9 reshape_reshape.14
  28.0 2.6 reshape_reshape.12
  30.6 4.9 multiply_bitcast_fusion
  35.5 339.6 %while.17 = (s32[]{:T(128)}, f32[4,64,64]{2,1,0:T(8,128)S(1)}, bf16[4,64,64]{1,2,0:T(8,128)(2,1)S(1)}, f32[12,4,64,64]{3,2,1,0:T(8,128)}, bf16[12,4,64,64]{3,2,1...) while((s32[]{:T(128)}, f32[4,64,64]{2,1,0:T(8,128)S(1)}, ...), condition=%wide.region_3.4_spmd.clone, body=%wide.region_1.3_spmd.clone.sunk | while | flops 58290240 | bytes 4974245 | solution.py:189
  37.6 1.0 constant_dynamic-slice_fusion.12
  40.6 19.7 %custom-call.9 = f32[4,1,64,64]{2,3,1,0:T(8,128)S(1)} custom-call(f32[4,1,64,64]{3,2,1,0:T(8,128)S(1)} %fusion.259), custom_call_target="InvertDiagBlocksLowerTriangular" | custom-call | tf_op jit(solution)/shard_map/while/body/eval_jaxpr/jit(_solve_triangular)/vmap()/triangular_solve | solution.py:99
  65.9 1.0 constant_dynamic-slice_fusion.12
  68.9 19.7 %custom-call.9 = f32[4,1,64,64]{2,3,1,0:T(8,128)S(1)} custom-call(f32[4,1,64,64]{3,2,1,0:T(8,128)S(1)} %fusion.259), custom_call_target="InvertDiagBlocksLowerTriangular" | custom-call | tf_op jit(solution)/shard_map/while/body/eval_jaxpr/jit(_solve_triangular)/vmap()/triangular_solve | solution.py:99
  94.2 1.0 constant_dynamic-slice_fusion.12
  97.2 19.7 %custom-call.9 = f32[4,1,64,64]{2,3,1,0:T(8,128)S(1)} custom-call(f32[4,1,64,64]{3,2,1,0:T(8,128)S(1)} %fusion.259), custom_call_target="InvertDiagBlocksLowerTriangular" | custom-call | tf_op jit(solution)/shard_map/while/body/eval_jaxpr/jit(_solve_triangular)/vmap()/triangular_solve | solution.py:99
  122.5 1.0 constant_dynamic-slice_fusion.12
  125.5 19.7 %custom-call.9 = f32[4,1,64,64]{2,3,1,0:T(8,128)S(1)} custom-call(f32[4,1,64,64]{3,2,1,0:T(8,128)S(1)} %fusion.259), custom_call_target="InvertDiagBlocksLowerTriangular" | custom-call | tf_op jit(solution)/shard_map/while/body/eval_jaxpr/jit(_solve_triangular)/vmap()/triangular_solve | solution.py:99
  150.8 1.0 constant_dynamic-slice_fusion.12
  153.8 19.7 %custom-call.9 = f32[4,1,64,64]{2,3,1,0:T(8,128)S(1)} custom-call(f32[4,1,64,64]{3,2,1,0:T(8,128)S(1)} %fusion.259), custom_call_target="InvertDiagBlocksLowerTriangular" | custom-call | tf_op jit(solution)/shard_map/while/body/eval_jaxpr/jit(_solve_triangular)/vmap()/triangular_solve | solution.py:99
  179.1 1.0 constant_dynamic-slice_fusion.12
  182.0 19.7 %custom-call.9 = f32[4,1,64,64]{2,3,1,0:T(8,128)S(1)} custom-call(f32[4,1,64,64]{3,2,1,0:T(8,128)S(1)} %fusion.259), custom_call_target="InvertDiagBlocksLowerTriangular" | custom-call | tf_op jit(solution)/shard_map/while/body/eval_jaxpr/jit(_solve_triangular)/vmap()/triangular_solve | solution.py:99
  210.4 19.7 %custom-call.9 = f32[4,1,64,64]{2,3,1,0:T(8,128)S(1)} custom-call(f32[4,1,64,64]{3,2,1,0:T(8,128)S(1)} %fusion.259), custom_call_target="InvertDiagBlocksLowerTriangular" | custom-call | tf_op jit(solution)/shard_map/while/body/eval_jaxpr/jit(_solve_triangular)/vmap()/triangular_solve | solution.py:99
  238.6 19.7 %custom-call.9 = f32[4,1,64,64]{2,3,1,0:T(8,128)S(1)} custom-call(f32[4,1,64,64]{3,2,1,0:T(8,128)S(1)} %fusion.259), custom_call_target="InvertDiagBlocksLowerTriangular" | custom-call | tf_op jit(solution)/shard_map/while/body/eval_jaxpr/jit(_solve_triangular)/vmap()/triangular_solve | solution.py:99
  266.9 19.7 %custom-call.9 = f32[4,1,64,64]{2,3,1,0:T(8,128)S(1)} custom-call(f32[4,1,64,64]{3,2,1,0:T(8,128)S(1)} %fusion.259), custom_call_target="InvertDiagBlocksLowerTriangular" | custom-call | tf_op jit(solution)/shard_map/while/body/eval_jaxpr/jit(_solve_triangular)/vmap()/triangular_solve | solution.py:99
  295.2 19.7 %custom-call.9 = f32[4,1,64,64]{2,3,1,0:T(8,128)S(1)} custom-call(f32[4,1,64,64]{3,2,1,0:T(8,128)S(1)} %fusion.259), custom_call_target="InvertDiagBlocksLowerTriangular" | custom-call | tf_op jit(solution)/shard_map/while/body/eval_jaxpr/jit(_solve_triangular)/vmap()/triangular_solve | solution.py:99
  323.5 19.7 %custom-call.9 = f32[4,1,64,64]{2,3,1,0:T(8,128)S(1)} custom-call(f32[4,1,64,64]{3,2,1,0:T(8,128)S(1)} %fusion.259), custom_call_target="InvertDiagBlocksLowerTriangular" | custom-call | tf_op jit(solution)/shard_map/while/body/eval_jaxpr/jit(_solve_triangular)/vmap()/triangular_solve | solution.py:99
  351.8 19.7 %custom-call.9 = f32[4,1,64,64]{2,3,1,0:T(8,128)S(1)} custom-call(f32[4,1,64,64]{3,2,1,0:T(8,128)S(1)} %fusion.259), custom_call_target="InvertDiagBlocksLowerTriangular" | custom-call | tf_op jit(solution)/shard_map/while/body/eval_jaxpr/jit(_solve_triangular)/vmap()/triangular_solve | solution.py:99
  375.1 1.1 copy.77
  377.6 2.2 copy.74
  379.8 1.4 reshape.108
  381.2 1.9 copy.75
  384.4 12.5 %all-gather = bf16[16,64,64]{2,1,0:T(8,128)(2,1)S(1)} all-gather(bf16[4,64,64]{2,1,0:T(8,128)(2,1)S(1)} %copy-done.15), channel_id=2, replica_groups=mesh['sp_0'=8,'sp_1'=4,'tp'=8] {'sp_1'}, dimensions={0}, use_global_device_ids=true | all-gather | bytes 163840 | tf_op jit(solution)/shard_map/all_gather | solution.py:34
  397.0 12.2 %all-gather.2 = bf16[16,64,64]{2,1,0:T(8,128)(2,1)S(1)} all-gather(bf16[4,64,64]{2,1,0:T(8,128)(2,1)S(1)} %copy-done.13), channel_id=4, replica_groups=mesh['sp_0'=8,'sp_1'=4,'tp'=8] {'sp_1'}, dimensions={0}, use_global_device_ids=true | all-gather | bytes 163840 | tf_op jit(solution)/shard_map/all_gather | solution.py:34
  409.8 29.2 %all-gather.3 = bf16[32,64,64]{2,1,0:T(8,128)(2,1)S(1)} all-gather(bf16[4,64,64]{2,1,0:T(8,128)(2,1)S(1)} %convolution_add_fusion.10), channel_id=5, replica_groups=mesh['sp_0'=8,'sp_1'=4,'tp'=8] {'sp_0'}, dimensions={0}, use_global_device_ids=true | all-gather | bytes 294912 | tf_op jit(solution)/shard_map/all_gather | solution.py:34
  441.3 25.5 %all-gather.1 = bf16[32,64,64]{2,1,0:T(8,128)(2,1)S(1)} all-gather(bf16[4,64,64]{2,1,0:T(8,128)(2,1)S(1)} %fusion.143), channel_id=3, replica_groups=mesh['sp_0'=8,'sp_1'=4,'tp'=8] {'sp_0'}, dimensions={0}, use_global_device_ids=true | all-gather | bytes 294912 | tf_op jit(solution)/shard_map/all_gather | solution.py:34
  470.1 2.0 fusion.73
  472.1 1.2 fusion.160
  475.6 42.6 %all_to_all.10 = bf16[8,96,2048]{2,1,0:T(8,128)(2,1)} all-to-all(bf16[8,96,2048]{2,1,0:T(8,128)(2,1)S(1)} %bitcast.167), channel_id=1, replica_groups=mesh['sp_0'=8,'sp_1'=4,'tp'=8] {'tp'}, dimensions={0} | all-to-all | bytes 6291456 | tf_op jit(solution)/shard_map/all_to_all | solution.py:56
  518.2 2.5 reduce_sum.61
  521.5 41.7 %all_to_all.11 = bf16[8,96,2048]{2,1,0:T(8,128)(2,1)} all-to-all(bf16[8,96,2048]{2,1,0:T(8,128)(2,1)S(1)} %stack.2), channel_id=1, replica_groups=mesh['sp_0'=8,'sp_1'=4,'tp'=8] {'tp'}, dimensions={0} | all-to-all | bytes 6291456 | tf_op jit(solution)/shard_map/all_to_all | solution.py:234
  563.3 6.6 %fusion.62 = f32[768,640]{1,0:T(8,128)} fusion(bf16[768,2048]{1,0:T(8,128)(2,1)} %bitcast.171, bf16[2048,1920]{1,0:T(8,128)(2,1)} %all-gather.6.cloned.1.call-done), kind=kOutput, calls=%fused_computation.87 | convolution fusion | flops 2013265920 | bytes 7733248 | tf_op jit(solution)/shard_map/dot_general | solution.py:236
  569.8 11.6 %convolution_convert_fusion = bf16[768,2048]{1,0:T(8,128)(2,1)} fusion(bf16[2048,1920]{1,0:T(8,128)(2,1)} %all-gather.6.cloned.1.call-done, f32[768,640]{1,0:T(8,128)} %fusion.62, bf16[768,2048]{1,0:T(8,128)(2,1)} %bitcast.172), kind=kOutput, calls=%fused_computation.82 | convolution fusion | flops 4031053824 | bytes 13500416 | tf_op jit(solution)/shard_map/dot_general | solution.py:241
  581.4 35.8 %reduce-scatter.2.cloned.1.call-done = bf16[96,2048]{1,0:T(8,128)(2,1)} async-done(((bf16[768,2048]{1,0:T(8,128)(2,1)}), bf16[96,2048]{1,0:T(8,128)(2,1)}) %reduce-scatter.2.cloned.1.call-update) | async-done | bytes 393232 | tf_op jit(solution)/shard_map/reduce_scatter | solution.py:240
  617.2 1.9 add_convert_fusion
  (421 shorter events, 110.6 us)
Async XLA Ops:
  6.5 467.8 %copy-start = (bf16[256,2048]{1,0:T(8,128)(2,1)S(1)}, bf16[256,2048]{1,0:T(8,128)(2,1)}, u32[]{:S(2)}) copy-start(bf16[256,2048]{1,0:T(8,128)(2,1)} %param.29) | copy-start | bytes 3145732
  6.5 556.7 %all-gather.6.cloned.1.call-start = ((), (), s32[]{:S(2)}) async-start(), calls=%async_computation.3 | async-start | bytes 8110080 | tf_op jit(solution)/shard_map/all_gather | solution.py:18
  8.3 608.8 %reduce-scatter.2.cloned.1.call-start = ((), (), s32[]{:S(2)}) async-start(), calls=%async_computation.4 | async-start | bytes 3538944 | tf_op jit(solution)/shard_map/reduce_scatter | solution.py:240
  9.6 3.2 copy-start.9
  9.6 3.2 copy-start.27
  11.8 4.4 copy-start.23
  19.0 6.0 copy-start.1
  30.6 4.9 copy-start.21
  35.5 339.6 %copy-start.7 = (bf16[768,256]{1,0:T(8,128)(2,1)S(1)}, bf16[768,256]{1,0:T(8,128)(2,1)}, u32[]{:S(2)}) copy-start(bf16[768,256]{1,0:T(8,128)(2,1)} %param.21) | copy-start | bytes 1179652
  381.2 2.6 copy-start.26
  381.2 3.2 copy-start.15
  381.2 15.7 %copy-start.13 = (bf16[4,64,64]{2,1,0:T(8,128)(2,1)S(1)}, bf16[4,64,64]{2,1,0:T(8,128)(2,1)}, u32[]{:S(2)}) copy-start(bf16[4,64,64]{2,1,0:T(8,128)(2,1)} %convert_element_type.170) | copy-start | bytes 98308
  439.1 0.6 copy-start.14
  439.9 0.6 copy-start.10
  440.5 0.6 copy-start.11
  441.3 27.9 %copy-start.12 = (bf16[4,64,64]{2,1,0:T(8,128)(2,1)}, bf16[4,64,64]{2,1,0:T(8,128)(2,1)S(1)}, u32[]{:S(2)}) copy-start(bf16[4,64,64]{2,1,0:T(8,128)(2,1)S(1)} %fusion.143) | copy-start | bytes 98308
  441.3 30.8 %copy-start.5 = (f32[768,4,64]{0,2,1:T(8,128)S(1)}, f32[768,4,64]{0,2,1:T(8,128)}, u32[]{:S(2)}) copy-start(f32[768,4,64]{0,2,1:T(8,128)} %reshape.108) | copy-start | bytes 2359300
  466.8 2.4 copy-start.6
  467.0 0.7 copy-start.22
  467.8 1.4 copy-start.16
  468.0 1.3 copy-start.17
  468.1 1.1 copy-start.18
  468.3 1.0 copy-start.19
  468.4 0.8 copy-start.20
  470.1 3.4 copy-start.2
  472.1 1.4 copy-start.4
  472.1 1.4 copy-start.25
  473.6 1.0 copy-start.8
  518.2 2.5 copy-start.3
  518.2 2.8 copy-start.24
Sparse Core Ops, SparseCore 0:
  9.9 97.6 all-gather.5
  581.5 35.5 reduce-scatter.1
